TPU v7x, 32 devices: a whole 2x2x4 slice. The times are simulated.
32 devices in a mesh: gr: 2 (over x), sp: 8 (over z, y), tp: 2 (over core).
Axes of the slice: x: 2, y: 2, z: 4, core: 2. Of those that a mesh axis runs over, the one named last changes fastest.
Arguments:
- inputs: bfloat16 [4096, 2048], P(('gr', 'sp'), 'tp'), parts along dimension 0, may hold values from -6 to 6
- x_weight: bfloat16 [2048, 4096], P(None, 'tp'), may hold values from -0.125 to 0.125
- b_weight: bfloat16 [2048, 2048], P(None, 'tp'), may hold values from -0.125 to 0.125
- dt_weight: bfloat16 [2048, 128], replicated, may hold values from -0.125 to 0.125
- dt_bias: float32 [2, 64], replicated, may hold values from -2 to -1
- decay_rate: float32 [2, 64], replicated, may hold values from 0.3 to 10
- conv_x: bfloat16 [5, 4096], P(None, 'tp'), may hold values from -2.5 to 2.5
- conv_b: bfloat16 [5, 2048], P(None, 'tp'), may hold values from -2.5 to 2.5
- query_c: bfloat16 [2, 16, 128], P('gr', 'tp'), parts along dimension 0, may hold values from -6 to 6
- query_gate: bfloat16 [2, 64, 64], P('gr', 'tp'), parts along dimension 0, may hold values from -6 to 6
- read_span: int32 [2], P('gr'), parts along dimension 0, may hold values from 0 to 15
- read_gain: float32 [64, 64], P('tp'), may hold values from 0.1 to 1.9
Outputs:
- span_cache: bfloat16 [32, 2, 64, 8192], P('gr', None, 'tp', 'sp'), parts along dimension 0
- first_read: bfloat16 [2, 64, 64], P('gr', 'tp'), parts along dimension 0
There are 2 independent parts, one for each index of `gr`. A program takes and returns all parts, laid end to end along the dimension named above; an argument that names none is the same for every part. Nothing has to cross between parts.
Inputs may be any that keep to these rules, and one draw needn't show every extreme that they name: read_span holds one span index from 0 to 15.
All inputs are finite; a program needn't handle non-finite values.
Results may differ from a plain program's by a relative error of at most 0.009.
Values may be sent and summed in bfloat16 or wider, within the bound.
A program may use at most 64 MiB of HBM per device.

v0:
```python
import jax
import jax.numpy as jnp
from jax import lax
from jax.sharding import PartitionSpec as P

H = 64
P_SIZE = 64
G = 16
N = 128
KW = 5
SPAN = 128
EPSILON = 1e-06


def extended(shard, sides, width):
    for axis, dim in sides:
        size, length = (lax.axis_size(axis), shard.shape[dim])
        up = [(i, (i + 1) % size) for i in range(size - 1)]
        down = [(j, i) for i, j in up]
        last = lax.slice_in_dim(shard, length - width, length, axis=dim)
        initial = lax.slice_in_dim(shard, 0, width, axis=dim)
        before = lax.ppermute(last, axis, up)
        after = lax.ppermute(initial, axis, down)
        shard = jnp.concatenate([before, shard, after], axis=dim)
    return shard


def span_states(value_rows, key_rows, step_sizes, log_decay):
    running = jnp.cumsum(log_decay, axis=1)
    closing = running[:, -1]
    forward = jnp.exp(closing[:, None, 0] - running[:, :, 0]) * step_sizes[:, :, 0]
    backward = jnp.exp(running[:, :, 1] - log_decay[:, :, 1]) * step_sizes[:, :, 1]
    weights = jnp.stack([forward, backward], axis=2)
    states = jnp.einsum(
        "kseh,kshn,kshp->kehnp",
        weights,
        key_rows.astype(jnp.float32),
        value_rows.astype(jnp.float32),
    )
    return (states, closing)


def read_weights(span_logs, chosen):
    span_count = span_logs.shape[0]
    ahead_sum = jnp.cumsum(span_logs[:, 0], axis=0)
    behind = jnp.flip(jnp.cumsum(jnp.flip(span_logs[:, 1], 0), axis=0), 0)
    positions = jnp.arange(span_count, dtype=jnp.int32)[:, None]
    ahead_pick = lax.dynamic_slice_in_dim(ahead_sum, chosen, 1, 0)
    behind_pick = lax.dynamic_slice_in_dim(behind, chosen, 1, 0)
    before = positions <= chosen
    after = positions >= chosen
    forward = jnp.where(before, jnp.exp(jnp.where(before, ahead_pick - ahead_sum, 0.0)), 0.0)
    backward = jnp.where(after, jnp.exp(jnp.where(after, behind_pick - behind, 0.0)), 0.0)
    return jnp.stack([forward, backward], axis=1)


def per_device(
    inputs,
    x_weight,
    b_weight,
    dt_weight,
    dt_bias,
    decay_rate,
    conv_x,
    conv_b,
    query_c,
    query_gate,
    read_span,
    read_gain,
):
    tokens = inputs.shape[0]
    heads_local = x_weight.shape[1] // P_SIZE
    per_group = H // G
    tp_index = lax.axis_index("tp")
    sp_index = lax.axis_index("sp")
    dt_local = lax.dynamic_slice_in_dim(
        dt_weight.reshape(dt_weight.shape[0], 2, H), tp_index * heads_local, heads_local, 2
    )
    dt_local = dt_local.reshape(dt_weight.shape[0], 2 * heads_local)
    slab_piece = lax.all_gather(inputs, "tp", axis=1, tiled=True)
    x_part = jnp.dot(slab_piece, x_weight, preferred_element_type=jnp.float32)
    b_part = jnp.dot(slab_piece, b_weight, preferred_element_type=jnp.float32)
    dt_part = jnp.dot(slab_piece, dt_local, preferred_element_type=jnp.float32)
    joined = jnp.concatenate([x_part.astype(jnp.bfloat16), b_part.astype(jnp.bfloat16)], axis=1)
    reach = KW // 2
    padded = extended(joined, (("sp", 0),), reach)
    taps = jnp.concatenate([conv_x, conv_b], axis=1)
    mixed_rows = jnp.zeros(joined.shape, jnp.float32)
    for offset in range(KW):
        mixed_rows = mixed_rows + taps[offset].astype(jnp.float32) * padded[
            offset : offset + tokens
        ].astype(jnp.float32)
    mixed_rows = jax.nn.silu(mixed_rows).astype(jnp.bfloat16)
    split_at = x_weight.shape[1]
    values = mixed_rows[:, :split_at]
    key_rows = mixed_rows[:, split_at:]
    length = tokens * lax.axis_size("sp")
    bias_local = lax.dynamic_slice_in_dim(dt_bias, tp_index * heads_local, heads_local, 1)
    rate_local = lax.dynamic_slice_in_dim(decay_rate, tp_index * heads_local, heads_local, 1)
    dt_raw = dt_part.astype(jnp.bfloat16).reshape(tokens, 2, heads_local)
    step_sizes = jax.nn.softplus(dt_raw.astype(jnp.float32) + bias_local)
    log_decay = -(step_sizes * rate_local) / length
    span_count = tokens // SPAN
    value_rows = values.reshape(span_count, SPAN, heads_local, P_SIZE)
    group_keys = key_rows.reshape(span_count, SPAN, heads_local // per_group, N)
    group_keys = jnp.repeat(group_keys, per_group, axis=2)
    states, closing = span_states(
        value_rows,
        group_keys,
        step_sizes.reshape(span_count, SPAN, 2, heads_local),
        log_decay.reshape(span_count, SPAN, 2, heads_local),
    )
    local_rows = states.reshape(span_count, 2, heads_local, N * P_SIZE).astype(jnp.bfloat16)
    all_logs = lax.all_gather(closing, "sp", axis=0, tiled=True)
    weights = read_weights(all_logs, read_span[0])
    cache_rows = lax.all_to_all(local_rows, "sp", split_axis=3, concat_axis=0, tiled=True)
    columns = cache_rows.shape[3] // P_SIZE
    gathered = jnp.einsum("jeh,jehx->hx", weights, cache_rows.astype(jnp.float32)).reshape(
        heads_local, columns, P_SIZE
    )
    picked = lax.dynamic_slice_in_dim(query_c[0], sp_index * columns, columns, 1)
    query_cols = jnp.repeat(picked.astype(jnp.float32), per_group, axis=0)
    partial_read = jnp.einsum("hnp,hn->hp", gathered, query_cols)
    read_total = lax.psum(partial_read, "sp")
    gated_read = read_total * jax.nn.silu(query_gate[0].astype(jnp.float32))
    square_sum = lax.psum(jnp.sum(gated_read * gated_read), "tp")
    mean_square = square_sum / (H * P_SIZE)
    first_read = (gated_read * lax.rsqrt(mean_square + EPSILON) * read_gain)[None].astype(
        jnp.bfloat16
    )
    return (cache_rows, first_read)


def solution(mesh):
    return jax.shard_map(
        per_device,
        mesh=mesh,
        in_specs=(
            P(("gr", "sp"), "tp"),
            P(None, "tp"),
            P(None, "tp"),
            P(),
            P(),
            P(),
            P(None, "tp"),
            P(None, "tp"),
            P("gr", "tp", None),
            P("gr", "tp", None),
            P("gr"),
            P("tp", None),
        ),
        out_specs=(P("gr", None, "tp", "sp"), P("gr", "tp", None)),
        check_vma=False,
    )
```

profile of v0, /device:TPU:0, one launch (start us, length us, event | category | flops | bytes accessed | tf_op | source)
XLA Modules:
  0.0 222.9 jit_solution(17773302501208012883)
XLA Ops:
  7.2 0.7 all-gather.3.cloned.1.call-update
  7.9 0.8 constant_dynamic-update-slice_fusion.1
  8.7 0.8 constant_dynamic-slice_fusion.2
  9.4 1.2 copy.63
  10.7 0.7 constant_dynamic-update-slice_fusion
  11.5 9.8 %all-gather.3.cloned.1.call-done = bf16[256,2048]{1,0:T(8,128)(2,1)} async-done(((bf16[256,1024]{1,0:T(8,128)(2,1)}), bf16[256,2048]{1,0:T(8,128)(2,1)}) %all-gather.3.cloned.1.call-update) | async-done | bytes 1048592 | tf_op jit(solution)/shard_map/all_gather | solution.py:80
  21.3 1.8 fusion.9
  23.2 0.2 copy.65
  23.5 0.2 fusion.24
  23.9 5.9 %convolution_convert_fusion = bf16[256,2048]{1,0:T(8,128)(2,1)S(1)} fusion(bf16[256,2048]{1,0:T(8,128)(2,1)S(1)} %copy-done.1, bf16[2048,2048]{1,0:T(8,128)(2,1)} %param.13), kind=kOutput, calls=%fused_computation.3 | convolution fusion | flops 2148007936 | bytes 10485760 | tf_op jit(solution)/shard_map/dot_general | solution.py:81
  29.8 1.3 convolution_convert_fusion.1
  31.1 3.6 %collective-permute-start = (bf16[2,3072]{1,0:T(2,128)(2,1)S(1)}, bf16[2,3072]{1,0:T(2,128)(2,1)S(1)}, u32[]{:S(2)}, u32[]{:S(2)}) collective-permute-start(bf16[2,3072]{1,0:T(2,128)(2,1)S(1)} %get-tuple-element.6), channel_id=1, source_target_pairs={{0,2},{2,4},{4,6},{6,8},{8,10},{10,12},{12,14},{1,3},{3,5},{5,7},{... | collective-permute-start | bytes 36872 | tf_op jit(solution)/shard_map/ppermute | solution.py:22
  34.8 1.3 collective-permute-start.1
  36.3 4.1 %collective-permute-done.1 = bf16[2,3072]{1,0:T(2,128)(2,1)S(1)} collective-permute-done((bf16[2,3072]{1,0:T(2,128)(2,1)S(1)}, bf16[2,3072]{1,0:T(2,128)(2,1)S(1)}, u32[]{:S(2)}, u32[]{:S(2)}) %collective-permute-start.1) | collective-permute-done | bytes 12320 | tf_op jit(solution)/shard_map/ppermute | solution.py:23
  40.4 0.5 maximum_maximum_fusion
  40.9 2.9 %multiply_convert_fusion = bf16[256,3072]{1,0:T(8,128)(2,1)S(1)} fusion(bf16[256,1024]{1,0:T(8,128)(2,1)S(1)} %convolution_convert_fusion.1, bf16[256,2048]{1,0:T(8,128)(2,1)S(1)} %convolution_convert_fusion, bf16[258,3072]{1,0:T(8,128)(2,1)S(1)} %get-tuple-element.5, bf16[258,3072]{1,0:T(8,128)(2,1)S(1)} %get-tuple-element.4, f32[3072]{0:T(1024)S(1)} %bitcast.103, ...), kind=kLoop, calls=%fused_computation.2 | loop fusion | flops 17301504 | bytes 9498624 | tf_op jit(solution)/shard_map/convert_element_type | solution.py:93
  43.7 0.2 slice_convert_fusion
  44.0 3.0 %reshape.152 = f32[2,128,32,64]{3,2,1,0:T(8,128)} reshape(f32[256,2048]{1,0:T(8,128)S(1)} %slice_convert_fusion) | data formatting | bytes 4194304 | tf_op jit(solution)/shard_map/convert.7
  47.0 3.8 %copy.62 = f32[2,128,32,64]{1,3,2,0:T(8,128)S(1)} copy(f32[2,128,32,64]{3,2,1,0:T(8,128)} %reshape.152) | data formatting | bytes 4194304 | tf_op jit(solution)/shard_map/convert.7
  51.0 0.6 broadcast_in_dim.43
  51.6 2.0 convert_bitcast_fusion
  53.6 14.1 %copy.82 = bf16[2,2,32,128,64]{2,1,0,4,3:T(2,128)(2,1)} copy(bf16[2,2,32,128,64]{3,4,1,2,0:T(8,128)(2,1)} %convert_bitcast_fusion) | data formatting | bytes 4194304 | tf_op jit(solution)/shard_map/convert_element_type | solution.py:113
  67.7 11.2 %reshape.153 = bf16[8,2,65536]{2,1,0:T(2,128)(2,1)} reshape(bf16[8192,2,2,32]{3,2,1,0:T(2,128)(2,1)} %bitcast.92) | data formatting | bytes 4194304
  78.9 5.6 %all-to-all-start = ((bf16[8,2,65536]{2,1,0:T(2,128)(2,1)}), bf16[8,2,65536]{2,1,0:T(2,128)(2,1)S(1)}, u32[]{:S(2)}, u32[]{:S(2)}) async-start(bf16[8,2,65536]{2,1,0:T(2,128)(2,1)} %reshape.153), calls=%async_computation | async-start | bytes 4194304 | tf_op jit(solution)/shard_map/all_to_all | solution.py:116
  85.2 65.2 %all-gather = f32[16,1,2,32]{3,2,1,0:T(2,128)S(1)} all-gather(f32[2,1,2,32]{3,2,1,0:T(2,128)S(1)} %get-tuple-element.8), channel_id=2, replica_groups=mesh['gr'=2,'sp'=8,'tp'=2] {'sp'}, dimensions={0}, use_global_device_ids=true | all-gather | bytes 4608 | tf_op jit(solution)/shard_map/all_gather | solution.py:114
  150.8 6.6 %reshape.154 = bf16[8192,2,2,32]{3,2,1,0:T(2,128)(2,1)} reshape(bf16[8,2,65536]{2,1,0:T(2,128)(2,1)S(1)} %all-to-all-done) | data formatting | bytes 4194304
  157.4 17.8 %copy.84 = bf16[2,2,32,8,1024]{4,2,1,0,3:T(8,128)(2,1)S(1)} copy(bf16[2,2,32,8,1024]{2,1,0,4,3:T(2,128)(2,1)} %bitcast.93) | data formatting | bytes 4194304 | tf_op jit(solution)/shard_map/all_to_all | solution.py:116
  175.2 2.4 %fusion.2 = bf16[32,1,1024,1]{2,1,3,0:T(2,128)(2,1)S(1)} fusion(bf16[16,2,32,1]{0,3,1,2:T(2,128)(2,1)S(1)} %copy.75, bf16[16,2,32,1024]{3,2,1,0:T(8,128)(2,1)S(1)} %bitcast.95), kind=kOutput, calls=%fused_computation.7 | convolution fusion | flops 2097152 | bytes 2164736 | tf_op jit(solution)/shard_map/jeh,jehx->hx/dot_general | solution.py:118
  178.0 33.1 %psum.14 = f32[32,64]{1,0:T(8,128)S(1)} all-reduce(f32[32,64]{1,0:T(8,128)S(1)} %bitcast.110), channel_id=1, replica_groups=mesh['gr'=2,'sp'=8,'tp'=2] {'sp'}, use_global_device_ids=true, to_apply=%region_3.4 | all-reduce | flops 2048 | bytes 16384 | tf_op jit(solution)/shard_map/psum | solution.py:124
  211.0 0.6 multiply_reduce_fusion
  211.7 3.1 %psum.15 = f32[]{:T(128)} all-reduce(f32[]{:T(128)} %multiply_reduce_fusion), channel_id=1, replica_groups=mesh['gr'=2,'sp'=8,'tp'=2] {'tp'}, use_global_device_ids=true, to_apply=%region_5.6 | all-reduce | flops 1 | bytes 8 | tf_op jit(solution)/shard_map/psum | solution.py:126
  215.4 0.6 fusion.17
  (48 shorter events, 1.8 us)
Async XLA Ops:
  7.2 14.1 %all-gather.3.cloned.1.call-start = ((), (), s32[]{:S(2)}) async-start(), calls=%async_computation.1 | async-start | bytes 1572864 | tf_op jit(solution)/shard_map/all_gather | solution.py:80
  21.3 2.6 %copy-start.1 = (bf16[256,2048]{1,0:T(8,128)(2,1)S(1)}, bf16[256,2048]{1,0:T(8,128)(2,1)}, u32[]{:S(2)}) copy-start(bf16[256,2048]{1,0:T(8,128)(2,1)} %all-gather.3.cloned.1.call-done) | copy-start | bytes 3145732
  23.9 5.9 %copy-start.5 = (bf16[2048,1024]{1,0:T(8,128)(2,1)S(1)}, bf16[2048,1024]{1,0:T(8,128)(2,1)}, u32[]{:S(2)}) copy-start(bf16[2048,1024]{1,0:T(8,128)(2,1)} %param.14) | copy-start | bytes 12582916
  31.1 5.1 %collective-permute-start = (bf16[2,3072]{1,0:T(2,128)(2,1)S(1)}, bf16[2,3072]{1,0:T(2,128)(2,1)S(1)}, u32[]{:S(2)}, u32[]{:S(2)}) collective-permute-start(bf16[2,3072]{1,0:T(2,128)(2,1)S(1)} %get-tuple-element.6), channel_id=1, source_target_pairs={{0,2},{2,4},{4,6},{6,8},{8,10},{10,12},{12,14},{1,3},{3,5},{5,7},{... | collective-permute-start | bytes 36872 | tf_op jit(solution)/shard_map/ppermute | solution.py:22
  34.8 5.6 %collective-permute-start.1 = (bf16[2,3072]{1,0:T(2,128)(2,1)S(1)}, bf16[2,3072]{1,0:T(2,128)(2,1)S(1)}, u32[]{:S(2)}, u32[]{:S(2)}) collective-permute-start(bf16[2,3072]{1,0:T(2,128)(2,1)S(1)} %get-tuple-element.7), channel_id=1, source_target_pairs={{2,0},{4,2},{6,4},{8,6},{10,8},{12,10},{14,12},{3,1},{5,3},{7,5},{... | collective-permute-start | bytes 36872 | tf_op jit(solution)/shard_map/ppermute | solution.py:23
  78.8 6.3 %copy-start.4 = (bf16[1,8,128]{2,1,0:T(8,128)(2,1)S(1)}, bf16[1,8,128]{2,1,0:T(8,128)(2,1)}, u32[]{:S(2)}) copy-start(bf16[1,8,128]{2,1,0:T(8,128)(2,1)} %param.20) | copy-start | bytes 6148
  78.9 72.0 %all-to-all-start = ((bf16[8,2,65536]{2,1,0:T(2,128)(2,1)}), bf16[8,2,65536]{2,1,0:T(2,128)(2,1)S(1)}, u32[]{:S(2)}, u32[]{:S(2)}) async-start(bf16[8,2,65536]{2,1,0:T(2,128)(2,1)} %reshape.153), calls=%async_computation | async-start | bytes 4194304 | tf_op jit(solution)/shard_map/all_to_all | solution.py:116
  157.4 53.7 %copy-start.2 = (bf16[1,32,64]{2,1,0:T(8,128)(2,1)S(1)}, bf16[1,32,64]{2,1,0:T(8,128)(2,1)}, u32[]{:S(2)}) copy-start(bf16[1,32,64]{2,1,0:T(8,128)(2,1)} %param.21) | copy-start | bytes 12292
  175.2 40.9 %copy-start = (bf16[2,2,32,8,1024]{4,2,1,0,3:T(8,128)(2,1)}, bf16[2,2,32,8,1024]{4,2,1,0,3:T(8,128)(2,1)S(1)}, u32[]{:S(2)}) copy-start(bf16[2,2,32,8,1024]{4,2,1,0,3:T(8,128)(2,1)S(1)} %copy.84) | copy-start | bytes 6291460
  175.2 40.2 %copy-start.3 = (f32[32,64]{1,0:T(8,128)S(1)}, f32[32,64]{1,0:T(8,128)}, u32[]{:S(2)}) copy-start(f32[32,64]{1,0:T(8,128)} %param.23) | copy-start | bytes 24580
Sparse Core Ops, SparseCore 0:
  9.5 11.7 all-gather.2
where the time goes:
time: 224 us; the launch traced here: 223 us
  blocking collectives  101 us (45%)
  local copies, waits for them, and re-layouts  61.6 us (28%)
  between operations  15.7 us (7%)
  waiting for transfers between devices  14.6 us (7%)
  matrix products  13.5 us (6%)
  starting transfers between devices  10.6 us (5%)
  other arithmetic  5.54 us (2%)
    all_gather x1, blocking collectives, per_device(): all_logs = lax.all_gather(closing, 'sp', axis=0, tiled=True)  65.2 us
    psum x1, blocking collectives, per_device(): read_total = lax.psum(partial_read, 'sp')  33.1 us
    unnamed x20, local copies, waits for them, and re-layouts  20.1 us
    all_to_all x1, local copies, waits for them, and re-layouts, per_device(): lax.all_to_all(local_rows, 'sp', split_axis=3, concat_axis=0, tiled=True)  17.8 us
    convert_element_type x1, local copies, waits for them, and re-layouts, per_device(): states.reshape(span_count, 2, heads_local, N * P_SIZE).astype(jnp.bfloat16)  14.1 us
    all_gather x1, waiting for transfers between devices, per_device(): slab_piece = lax.all_gather(inputs, 'tp', axis=1, tiled=True)  9.82 us
    another operation x2, local copies, waits for them, and re-layouts  6.77 us
    dot_general x1, matrix products, per_device(): x_part = jnp.dot(slab_piece, x_weight, preferred_element_type=jnp.float32)  5.86 us
  transfers between devices with their start and end apart: 4, of which 2 were waited for; matrix products, arithmetic and copies ran while one was open for 2% of the time, Pallas kernels for 0%

commit v1 on v0

--- a/solution.py
+++ b/solution.py
@@ -121,7 +121,7 @@
     picked = lax.dynamic_slice_in_dim(query_c[0], sp_index * columns, columns, 1)
     query_cols = jnp.repeat(picked.astype(jnp.float32), per_group, axis=0)
     partial_read = jnp.einsum("hnp,hn->hp", gathered, query_cols)
-    read_total = lax.psum(partial_read, "sp")
+    read_total = jnp.sum(lax.all_gather(partial_read, "sp"), axis=0)
     gated_read = read_total * jax.nn.silu(query_gate[0].astype(jnp.float32))
     square_sum = lax.psum(jnp.sum(gated_read * gated_read), "tp")
     mean_square = square_sum / (H * P_SIZE)

time: 224 us -> 222 us (level)
    psum x1 -> x0, blocking collectives: 33.1 us -> none  [per_device(): read_total = lax.psum(partial_read, 'sp')]
    all_gather x0 -> x1, blocking collectives: none -> 30.5 us  [per_device(): read_total = jnp.sum(lax.all_gather(partial_read, 'sp'), axis=0)]
where the time goes in v1:
time: 222 us; the launch traced here: 220 us
  blocking collectives  98.8 us (45%)
  local copies, waits for them, and re-layouts  61.6 us (28%)
  between operations  15.7 us (7%)
  waiting for transfers between devices  14.6 us (7%)
  matrix products  13.5 us (6%)
  starting transfers between devices  10.6 us (5%)
  other arithmetic  5.56 us (3%)
    all_gather x1, blocking collectives, per_device(): all_logs = lax.all_gather(closing, 'sp', axis=0, tiled=True)  65.2 us
    all_gather x1, blocking collectives, per_device(): read_total = jnp.sum(lax.all_gather(partial_read, 'sp'), axis=0)  30.5 us
    unnamed x20, local copies, waits for them, and re-layouts  20.1 us
    all_to_all x1, local copies, waits for them, and re-layouts, per_device(): lax.all_to_all(local_rows, 'sp', split_axis=3, concat_axis=0, tiled=True)  17.8 us
    convert_element_type x1, local copies, waits for them, and re-layouts, per_device(): states.reshape(span_count, 2, heads_local, N * P_SIZE).astype(jnp.bfloat16)  14.1 us
    all_gather x1, waiting for transfers between devices, per_device(): slab_piece = lax.all_gather(inputs, 'tp', axis=1, tiled=True)  9.82 us
    another operation x2, local copies, waits for them, and re-layouts  6.77 us
    dot_general x1, matrix products, per_device(): x_part = jnp.dot(slab_piece, x_weight, preferred_element_type=jnp.float32)  5.86 us
  transfers between devices with their start and end apart: 4, of which 2 were waited for; matrix products, arithmetic and copies ran while one was open for 2% of the time, Pallas kernels for 0%

profile of v1, /device:TPU:0, one launch (start us, length us, event | category | flops | bytes accessed | tf_op | source)
XLA Modules:
  0.0 220.4 jit_solution(2304580302520683202)
XLA Ops:
  7.2 0.7 all-gather.4.cloned.1.call-update
  7.9 0.8 constant_dynamic-update-slice_fusion.1
  8.7 0.8 constant_dynamic-slice_fusion.2
  9.4 1.2 copy.79
  10.7 0.7 constant_dynamic-update-slice_fusion
  11.5 9.8 %all-gather.4.cloned.1.call-done = bf16[256,2048]{1,0:T(8,128)(2,1)} async-done(((bf16[256,1024]{1,0:T(8,128)(2,1)}), bf16[256,2048]{1,0:T(8,128)(2,1)}) %all-gather.4.cloned.1.call-update) | async-done | bytes 1048592 | tf_op jit(solution)/shard_map/all_gather | solution.py:80
  21.3 1.8 fusion.9
  23.2 0.2 copy.81
  23.5 0.2 fusion.24
  23.9 5.9 %convolution_convert_fusion = bf16[256,2048]{1,0:T(8,128)(2,1)S(1)} fusion(bf16[256,2048]{1,0:T(8,128)(2,1)S(1)} %copy-done.1, bf16[2048,2048]{1,0:T(8,128)(2,1)} %param.13), kind=kOutput, calls=%fused_computation.3 | convolution fusion | flops 2148007936 | bytes 10485760 | tf_op jit(solution)/shard_map/dot_general | solution.py:81
  29.8 1.3 convolution_convert_fusion.1
  31.1 3.6 %collective-permute-start = (bf16[2,3072]{1,0:T(2,128)(2,1)S(1)}, bf16[2,3072]{1,0:T(2,128)(2,1)S(1)}, u32[]{:S(2)}, u32[]{:S(2)}) collective-permute-start(bf16[2,3072]{1,0:T(2,128)(2,1)S(1)} %get-tuple-element.6), channel_id=1, source_target_pairs={{0,2},{2,4},{4,6},{6,8},{8,10},{10,12},{12,14},{1,3},{3,5},{5,7},{... | collective-permute-start | bytes 36872 | tf_op jit(solution)/shard_map/ppermute | solution.py:22
  34.8 1.3 collective-permute-start.1
  36.3 4.1 %collective-permute-done.1 = bf16[2,3072]{1,0:T(2,128)(2,1)S(1)} collective-permute-done((bf16[2,3072]{1,0:T(2,128)(2,1)S(1)}, bf16[2,3072]{1,0:T(2,128)(2,1)S(1)}, u32[]{:S(2)}, u32[]{:S(2)}) %collective-permute-start.1) | collective-permute-done | bytes 12320 | tf_op jit(solution)/shard_map/ppermute | solution.py:23
  40.4 0.5 maximum_maximum_fusion
  40.9 2.9 %multiply_convert_fusion = bf16[256,3072]{1,0:T(8,128)(2,1)S(1)} fusion(bf16[256,1024]{1,0:T(8,128)(2,1)S(1)} %convolution_convert_fusion.1, bf16[256,2048]{1,0:T(8,128)(2,1)S(1)} %convolution_convert_fusion, bf16[258,3072]{1,0:T(8,128)(2,1)S(1)} %get-tuple-element.5, bf16[258,3072]{1,0:T(8,128)(2,1)S(1)} %get-tuple-element.4, f32[3072]{0:T(1024)S(1)} %bitcast.105, ...), kind=kLoop, calls=%fused_computation.2 | loop fusion | flops 17301504 | bytes 9498624 | tf_op jit(solution)/shard_map/convert_element_type | solution.py:93
  43.7 0.2 slice_convert_fusion
  44.0 3.0 %reshape.153 = f32[2,128,32,64]{3,2,1,0:T(8,128)} reshape(f32[256,2048]{1,0:T(8,128)S(1)} %slice_convert_fusion) | data formatting | bytes 4194304 | tf_op jit(solution)/shard_map/convert.7
  47.0 3.8 %copy.78 = f32[2,128,32,64]{1,3,2,0:T(8,128)S(1)} copy(f32[2,128,32,64]{3,2,1,0:T(8,128)} %reshape.153) | data formatting | bytes 4194304 | tf_op jit(solution)/shard_map/convert.7
  51.0 0.6 broadcast_in_dim.43
  51.6 2.0 convert_bitcast_fusion
  53.6 14.1 %copy.98 = bf16[2,2,32,128,64]{2,1,0,4,3:T(2,128)(2,1)} copy(bf16[2,2,32,128,64]{3,4,1,2,0:T(8,128)(2,1)} %convert_bitcast_fusion) | data formatting | bytes 4194304 | tf_op jit(solution)/shard_map/convert_element_type | solution.py:113
  67.7 11.2 %reshape.154 = bf16[8,2,65536]{2,1,0:T(2,128)(2,1)} reshape(bf16[8192,2,2,32]{3,2,1,0:T(2,128)(2,1)} %bitcast.93) | data formatting | bytes 4194304
  78.9 5.6 %all-to-all-start = ((bf16[8,2,65536]{2,1,0:T(2,128)(2,1)}), bf16[8,2,65536]{2,1,0:T(2,128)(2,1)S(1)}, u32[]{:S(2)}, u32[]{:S(2)}) async-start(bf16[8,2,65536]{2,1,0:T(2,128)(2,1)} %reshape.154), calls=%async_computation | async-start | bytes 4194304 | tf_op jit(solution)/shard_map/all_to_all | solution.py:116
  85.2 65.2 %all-gather = f32[16,1,2,32]{3,2,1,0:T(2,128)S(1)} all-gather(f32[2,1,2,32]{3,2,1,0:T(2,128)S(1)} %get-tuple-element.8), channel_id=2, replica_groups=mesh['gr'=2,'sp'=8,'tp'=2] {'sp'}, dimensions={0}, use_global_device_ids=true | all-gather | bytes 4608 | tf_op jit(solution)/shard_map/all_gather | solution.py:114
  150.8 6.6 %reshape.155 = bf16[8192,2,2,32]{3,2,1,0:T(2,128)(2,1)} reshape(bf16[8,2,65536]{2,1,0:T(2,128)(2,1)S(1)} %all-to-all-done) | data formatting | bytes 4194304
  157.4 17.8 %copy.100 = bf16[2,2,32,8,1024]{4,2,1,0,3:T(8,128)(2,1)S(1)} copy(bf16[2,2,32,8,1024]{2,1,0,4,3:T(2,128)(2,1)} %bitcast.94) | data formatting | bytes 4194304 | tf_op jit(solution)/shard_map/all_to_all | solution.py:116
  175.2 2.4 %fusion.2 = bf16[32,1,1024,1]{2,1,3,0:T(2,128)(2,1)S(1)} fusion(bf16[16,2,32,1]{0,3,1,2:T(2,128)(2,1)S(1)} %copy.91, bf16[16,2,32,1024]{3,2,1,0:T(8,128)(2,1)S(1)} %bitcast.96), kind=kOutput, calls=%fused_computation.7 | convolution fusion | flops 2097152 | bytes 2164736 | tf_op jit(solution)/shard_map/jeh,jehx->hx/dot_general | solution.py:118
  178.0 30.5 %all-gather.1 = f32[256,64]{1,0:T(8,128)S(1)} all-gather(f32[32,64]{1,0:T(8,128)S(1)} %bitcast.111), channel_id=3, replica_groups=mesh['gr'=2,'sp'=8,'tp'=2] {'sp'}, dimensions={0}, use_global_device_ids=true | all-gather | bytes 73728 | tf_op jit(solution)/shard_map/all_gather | solution.py:124
  208.5 0.6 multiply_reduce_fusion
  209.1 3.1 %psum.7 = f32[]{:T(128)} all-reduce(f32[]{:T(128)} %multiply_reduce_fusion), channel_id=1, replica_groups=mesh['gr'=2,'sp'=8,'tp'=2] {'tp'}, use_global_device_ids=true, to_apply=%region_5.6 | all-reduce | flops 1 | bytes 8 | tf_op jit(solution)/shard_map/psum | solution.py:126
  212.9 0.6 fusion.17
  (49 shorter events, 1.8 us)
Async XLA Ops:
  7.2 14.1 %all-gather.4.cloned.1.call-start = ((), (), s32[]{:S(2)}) async-start(), calls=%async_computation.1 | async-start | bytes 1572864 | tf_op jit(solution)/shard_map/all_gather | solution.py:80
  21.3 2.6 %copy-start.1 = (bf16[256,2048]{1,0:T(8,128)(2,1)S(1)}, bf16[256,2048]{1,0:T(8,128)(2,1)}, u32[]{:S(2)}) copy-start(bf16[256,2048]{1,0:T(8,128)(2,1)} %all-gather.4.cloned.1.call-done) | copy-start | bytes 3145732
  23.9 5.9 %copy-start.5 = (bf16[2048,1024]{1,0:T(8,128)(2,1)S(1)}, bf16[2048,1024]{1,0:T(8,128)(2,1)}, u32[]{:S(2)}) copy-start(bf16[2048,1024]{1,0:T(8,128)(2,1)} %param.14) | copy-start | bytes 12582916
  31.1 5.1 %collective-permute-start = (bf16[2,3072]{1,0:T(2,128)(2,1)S(1)}, bf16[2,3072]{1,0:T(2,128)(2,1)S(1)}, u32[]{:S(2)}, u32[]{:S(2)}) collective-permute-start(bf16[2,3072]{1,0:T(2,128)(2,1)S(1)} %get-tuple-element.6), channel_id=1, source_target_pairs={{0,2},{2,4},{4,6},{6,8},{8,10},{10,12},{12,14},{1,3},{3,5},{5,7},{... | collective-permute-start | bytes 36872 | tf_op jit(solution)/shard_map/ppermute | solution.py:22
  34.8 5.6 %collective-permute-start.1 = (bf16[2,3072]{1,0:T(2,128)(2,1)S(1)}, bf16[2,3072]{1,0:T(2,128)(2,1)S(1)}, u32[]{:S(2)}, u32[]{:S(2)}) collective-permute-start(bf16[2,3072]{1,0:T(2,128)(2,1)S(1)} %get-tuple-element.7), channel_id=1, source_target_pairs={{2,0},{4,2},{6,4},{8,6},{10,8},{12,10},{14,12},{3,1},{5,3},{7,5},{... | collective-permute-start | bytes 36872 | tf_op jit(solution)/shard_map/ppermute | solution.py:23
  78.8 6.3 %copy-start.4 = (bf16[1,8,128]{2,1,0:T(8,128)(2,1)S(1)}, bf16[1,8,128]{2,1,0:T(8,128)(2,1)}, u32[]{:S(2)}) copy-start(bf16[1,8,128]{2,1,0:T(8,128)(2,1)} %param.20) | copy-start | bytes 6148
  78.9 72.0 %all-to-all-start = ((bf16[8,2,65536]{2,1,0:T(2,128)(2,1)}), bf16[8,2,65536]{2,1,0:T(2,128)(2,1)S(1)}, u32[]{:S(2)}, u32[]{:S(2)}) async-start(bf16[8,2,65536]{2,1,0:T(2,128)(2,1)} %reshape.154), calls=%async_computation | async-start | bytes 4194304 | tf_op jit(solution)/shard_map/all_to_all | solution.py:116
  175.2 38.4 %copy-start = (bf16[2,2,32,8,1024]{4,2,1,0,3:T(8,128)(2,1)}, bf16[2,2,32,8,1024]{4,2,1,0,3:T(8,128)(2,1)S(1)}, u32[]{:S(2)}) copy-start(bf16[2,2,32,8,1024]{4,2,1,0,3:T(8,128)(2,1)S(1)} %copy.100) | copy-start | bytes 6291460
  175.2 33.3 %copy-start.2 = (bf16[1,32,64]{2,1,0:T(8,128)(2,1)S(1)}, bf16[1,32,64]{2,1,0:T(8,128)(2,1)}, u32[]{:S(2)}) copy-start(bf16[1,32,64]{2,1,0:T(8,128)(2,1)} %param.21) | copy-start | bytes 12292
  175.2 37.7 %copy-start.3 = (f32[32,64]{1,0:T(8,128)S(1)}, f32[32,64]{1,0:T(8,128)}, u32[]{:S(2)}) copy-start(f32[32,64]{1,0:T(8,128)} %param.23) | copy-start | bytes 24580
Sparse Core Ops, SparseCore 0:
  9.5 11.7 all-gather.3
